TPU v7x, 32 devices: a whole 2x2x4 slice. The times are simulated.
32 devices in a mesh: sp: 8 (over z, core), tp: 4 (over y, x).
Axes of the slice: x: 2, y: 2, z: 4, core: 2. Of those that a mesh axis runs over, the one named last changes fastest.
Arguments:
- queries: bfloat16 [2048, 1024], P('sp', 'tp'), may hold values from -250 to 250
- keys_values: bfloat16 [2, 2048, 256], P(None, 'sp'), may hold values from -8 to 8
- sink_logits: float32 [16], P('tp'), may hold values from 1 to 5
- proj_weight: bfloat16 [1024, 2048], P('tp'), may hold values from -0.75 to 0.75
- residual: bfloat16 [2048, 2048], P('sp', 'tp'), may hold values from -6 to 6
- norm_gain: float32 [2048], replicated, may hold values from 0.1 to 1.9
- routes: int32 [2048, 2], P('sp'), may hold values from 0 to 7, all different within a row; in each aligned block of 256 rows (0 to 255, 256 to 511, ...) at most 128 rows name the same one
- route_weights: float32 [2048, 2], P('sp'), may hold values from 0.2 to 1
- gate_weight: bfloat16 [8, 2048, 2048], P('sp', None, 'tp'), may hold values from -0.125 to 0.125
- up_weight: bfloat16 [8, 2048, 2048], P('sp', None, 'tp'), may hold values from -0.125 to 0.125
- down_weight: bfloat16 [8, 2048, 2048], P('sp', None, 'tp'), may hold values from -0.125 to 0.125
- shared_gate: bfloat16 [2048, 2048], P(None, 'tp'), may hold values from -0.125 to 0.125
- shared_up: bfloat16 [2048, 2048], P(None, 'tp'), may hold values from -0.125 to 0.125
- shared_down: bfloat16 [2048, 2048], P(None, 'tp'), may hold values from -0.125 to 0.125
Outputs:
- output: bfloat16 [2048, 2048], P('sp', 'tp')
Inputs may be any that keep to these rules, and one draw needn't show every extreme that they name: `routes`: the 2 experts of a position differ. In each aligned block of 256 positions no expert is named by more than 128 positions, and in some block one expert is named by exactly 128.
All inputs are finite; a program needn't handle non-finite values.
Results may differ from a plain program's by a relative error of at most 0.0067.
Values may be sent and summed in bfloat16 or wider, within the bound.
A program may use at most 64 MiB of HBM per device.

v0:
```python
import jax
import jax.numpy as jnp
from jax import lax
from jax.sharding import PartitionSpec as P

D = 2048
HEADS = 16
KV_HEADS = 4
HEAD_WIDTH = 64
WINDOW = 128
TOP_K = 2
EXP_DEV = 1
TOK_DEV = 256
norm_eps = 1e-06


def passed_along(value, axis, steps):
    count = lax.axis_size(axis)
    initial, last = (max(0, -steps), min(count, count - steps))
    return lax.ppermute(value, axis, [(source, source + steps) for source in range(initial, last)])


def per_device(
    queries,
    keys_values,
    sink_logits,
    proj_weight,
    residual,
    norm_gain,
    routes,
    route_weights,
    gate_weight,
    up_weight,
    down_weight,
    shared_gate,
    shared_up,
    shared_down,
):
    tp_index = lax.axis_index("tp")
    sp_index = lax.axis_index("sp")
    sp_count = lax.axis_size("sp")
    tp_count = lax.axis_size("tp")
    heads_here = sink_logits.shape[0]
    col_width = residual.shape[1]
    blocks = TOK_DEV // WINDOW
    kv_group = HEADS // KV_HEADS
    earlier_keys = passed_along(keys_values[:, TOK_DEV - WINDOW :, :], "sp", 1)
    extended = jnp.concatenate([earlier_keys, keys_values], axis=1)
    extended = extended.reshape(2, TOK_DEV + WINDOW, KV_HEADS, HEAD_WIDTH)
    head_ids = tp_index * heads_here + jnp.arange(heads_here, dtype=jnp.int32)
    chosen = jnp.take(extended, head_ids // kv_group, axis=2)
    earlier = chosen[:, :TOK_DEV].reshape(2, blocks, WINDOW, heads_here, HEAD_WIDTH)
    later = chosen[:, WINDOW:].reshape(2, blocks, WINDOW, heads_here, HEAD_WIDTH)
    banded = jnp.concatenate([earlier, later], axis=2)
    query_blocks = queries.reshape(blocks, WINDOW, heads_here, HEAD_WIDTH)
    score_matrix = jnp.einsum(
        "bqhd,bkhd->bhqk", query_blocks, banded[0], preferred_element_type=jnp.float32
    ) * HEAD_WIDTH ** (-0.5)
    query_pos = jnp.arange(WINDOW, dtype=jnp.int32)[:, None]
    key_pos = jnp.arange(2 * WINDOW, dtype=jnp.int32)[None, :]
    distance = WINDOW + query_pos - key_pos
    absolute = (
        sp_index * TOK_DEV
        + jnp.arange(blocks, dtype=jnp.int32)[:, None, None] * WINDOW
        - WINDOW
        + key_pos[None]
    )
    allowed = (distance >= 0)[None] & (distance < WINDOW)[None] & (absolute >= 0)
    masked = jnp.where(allowed[:, None], score_matrix, -jnp.inf)
    sink_value = sink_logits[None, :, None, None]
    highest = jnp.maximum(jnp.max(masked, axis=-1, keepdims=True), sink_value)
    weights_exp = jnp.exp(masked - highest)
    denominator = jnp.sum(weights_exp, axis=-1, keepdims=True) + jnp.exp(sink_value - highest)
    softmax_weights = (weights_exp / denominator).astype(jnp.bfloat16)
    attended_values = jnp.einsum(
        "bhqk,bkhd->bqhd", softmax_weights, banded[1], preferred_element_type=jnp.float32
    )
    attended_values = attended_values.astype(jnp.bfloat16).reshape(TOK_DEV, heads_here * HEAD_WIDTH)
    attended_all = lax.all_gather(attended_values, "tp", axis=1, tiled=True)
    weight_rows = proj_weight.shape[0]
    column_share = lax.all_to_all(
        proj_weight.reshape(weight_rows, tp_count, col_width),
        "tp",
        split_axis=1,
        concat_axis=0,
        tiled=True,
    )
    column_share = column_share.reshape(HEADS * HEAD_WIDTH, col_width)
    feature_sum = jnp.dot(attended_all, column_share, preferred_element_type=jnp.float32)
    stream_cols = (feature_sum + residual.astype(jnp.float32)).astype(jnp.bfloat16)
    stream_rows = lax.all_gather(stream_cols, "tp", axis=1, tiled=True)
    gate_eff = (norm_gain[None, :, None] * gate_weight.astype(jnp.float32)).astype(jnp.bfloat16)
    up_eff = (norm_gain[None, :, None] * up_weight.astype(jnp.float32)).astype(jnp.bfloat16)
    shared_gate_eff = (norm_gain[:, None] * shared_gate.astype(jnp.float32)).astype(jnp.bfloat16)
    shared_up_eff = (norm_gain[:, None] * shared_up.astype(jnp.float32)).astype(jnp.bfloat16)
    experts_total = EXP_DEV * sp_count
    capacity = 2 * TOK_DEV * TOP_K // experts_total
    rows_per_expert = sp_count * capacity
    flat_routes = routes.reshape(-1)
    onehot = (flat_routes[:, None] == jnp.arange(experts_total, dtype=jnp.int32)[None, :]).astype(
        jnp.int32
    )
    before = jnp.cumsum(onehot, axis=0) - onehot
    slot_rank = jnp.sum(before * onehot, axis=1)
    slot_index = (
        flat_routes % EXP_DEV * rows_per_expert + flat_routes // EXP_DEV * capacity + slot_rank
    )
    token_of = jnp.arange(TOK_DEV * TOP_K, dtype=jnp.int32) // TOP_K
    slot_owner = (
        jnp.full((EXP_DEV * rows_per_expert,), TOK_DEV, jnp.int32).at[slot_index].set(token_of)
    )
    picked_rows = jnp.take(stream_rows, slot_owner, axis=0, mode="fill", fill_value=0)
    arrived = lax.all_to_all(
        picked_rows.reshape(EXP_DEV, sp_count, capacity, stream_rows.shape[1]),
        "sp",
        split_axis=1,
        concat_axis=1,
        tiled=True,
    )
    arrived = arrived.reshape(EXP_DEV, rows_per_expert, D)
    routed_squares = jnp.sum(jnp.square(arrived.astype(jnp.float32)), axis=-1)
    gate_sum = jnp.einsum("erd,edf->erf", arrived, gate_eff, preferred_element_type=jnp.float32)
    up_sum = jnp.einsum("erd,edf->erf", arrived, up_eff, preferred_element_type=jnp.float32)
    own_squares = jnp.sum(jnp.square(stream_rows.astype(jnp.float32)), axis=-1)
    shared_gate_sum = jnp.dot(stream_rows, shared_gate_eff, preferred_element_type=jnp.float32)
    shared_up_sum = jnp.dot(stream_rows, shared_up_eff, preferred_element_type=jnp.float32)
    routed_scale = lax.rsqrt(routed_squares / D + norm_eps)[..., None]
    own_scale = lax.rsqrt(own_squares / D + norm_eps)[:, None]
    hidden = (jax.nn.silu(routed_scale * gate_sum) * (routed_scale * up_sum)).astype(jnp.bfloat16)
    shared_hidden = (jax.nn.silu(own_scale * shared_gate_sum) * (own_scale * shared_up_sum)).astype(
        jnp.bfloat16
    )
    routed_piece = lax.all_gather(hidden, "tp", axis=2, tiled=True)
    own_piece = lax.all_gather(shared_hidden[None], "tp", axis=2, tiled=True)
    expert_out = jnp.einsum(
        "erf,efd->erd", routed_piece, down_weight, preferred_element_type=jnp.float32
    )
    shared_out = jnp.dot(own_piece[0], shared_down, preferred_element_type=jnp.float32)
    outgoing = expert_out.astype(jnp.bfloat16).reshape(EXP_DEV, sp_count, capacity, col_width)
    returned = lax.all_to_all(outgoing, "sp", split_axis=1, concat_axis=1, tiled=True).reshape(
        EXP_DEV * rows_per_expert, col_width
    )
    picked = jnp.take(returned, slot_index, axis=0).reshape(TOK_DEV, TOP_K, col_width)
    routed_sum = jnp.einsum("nk,nkd->nd", route_weights, picked.astype(jnp.float32))
    return (stream_cols.astype(jnp.float32) + shared_out + routed_sum).astype(jnp.bfloat16)


def solution(mesh):
    placed = (
        P("sp", "tp"),
        P(None, "sp", None),
        P("tp"),
        P("tp", None),
        P("sp", "tp"),
        P(),
        P("sp", None),
        P("sp", None),
        P("sp", None, "tp"),
        P("sp", None, "tp"),
        P("sp", None, "tp"),
        P(None, "tp"),
        P(None, "tp"),
        P(None, "tp"),
    )
    return jax.shard_map(
        per_device, mesh=mesh, in_specs=placed, out_specs=P("sp", "tp"), check_vma=False
    )
```

profile of v0, /device:TPU:0, one launch (start us, length us, event | category | flops | bytes accessed | tf_op | source)
XLA Modules:
  0.0 293.3 jit_solution(9455327325811044780)
XLA Ops:
  7.8 3.2 %collective-permute-start = (bf16[2,128,256]{1,2,0:T(8,128)(2,1)S(1)}, bf16[2,128,256]{1,2,0:T(8,128)(2,1)}, u32[]{:S(2)}, u32[]{:S(2)}) collective-permute-start(bf16[2,128,256]{1,2,0:T(8,128)(2,1)S(1)} %slice.34), channel_id=1, source_target_pairs={{0,4},{4,8},{8,12},{12,16},{16,20},{20,24},{24,28},{1,5},{5,9},{9,... | collective-permute-start | bytes 393224 | tf_op jit(solution)/shard_map/ppermute | solution.py:20
  11.0 2.3 copy.73
  13.3 4.5 %all-to-all-start = ((bf16[256,4,512]{0,2,1:T(8,128)(2,1)}), bf16[256,4,512]{0,2,1:T(8,128)(2,1)S(1)}, u32[]{:S(2)}, u32[]{:S(2)}) async-start(bf16[256,4,512]{0,2,1:T(8,128)(2,1)} %bitcast.91), calls=%async_computation | async-start | bytes 2097152 | tf_op jit(solution)/shard_map/all_to_all | solution.py:81
  20.7 1.4 gather_fusion
  27.6 1.5 fusion.48
  30.0 12.7 %all_gather.12 = bf16[256,1024]{0,1:T(8,128)(2,1)} all-gather(bf16[256,256]{0,1:T(8,128)(2,1)S(1)} %bitcast.95), channel_id=1, replica_groups=mesh['sp'=8,'tp'=4] {'tp'}, dimensions={1}, use_global_device_ids=true | all-gather | bytes 655360 | tf_op jit(solution)/shard_map/all_gather | solution.py:79
  42.7 1.3 copy.74
  44.0 2.6 fusion.25
  48.9 2.4 scatter_custom_fusion
  51.4 20.4 %all-gather.6.cloned.1.call-done = bf16[256,2048]{1,0:T(8,128)(2,1)} async-done(((bf16[256,512]{1,0:T(8,128)(2,1)}), bf16[256,2048]{1,0:T(8,128)(2,1)}) %all-gather.6.cloned.1.call-update) | async-done | bytes 1048592 | tf_op jit(solution)/shard_map/all_gather | solution.py:91
  71.8 10.2 %gather_fusion.1 = bf16[1024,2048]{1,0:T(8,128)(2,1)} fusion(bf16[256,2048]{1,0:T(8,128)(2,1)} %all-gather.6.cloned.1.call-done, s32[1024]{0:T(1024)S(1)} %fusion.39), kind=kCustom, calls=%fused_computation.1 | custom fusion | bytes 8392704 | tf_op jit(solution)/shard_map/jit(_take)/gather | solution.py:112
  82.0 2.5 broadcast_select_fusion
  84.5 98.4 %all_to_all.25 = bf16[1,8,128,2048]{3,2,0,1:T(8,128)(2,1)S(1)} all-to-all(bf16[1,8,128,2048]{3,2,0,1:T(8,128)(2,1)S(1)} %broadcast_select_fusion), channel_id=1, replica_groups=mesh['sp'=8,'tp'=4] {'sp'}, dimensions={1} | all-to-all | bytes 8388608 | tf_op jit(solution)/shard_map/all_to_all | solution.py:113
  184.5 2.4 fusion.3
  186.9 3.7 %multiply_convert_fusion.6 = bf16[1024,512]{1,0:T(8,128)(2,1)} fusion(f32[1024,512]{1,0:T(8,128)S(1)} %fusion.3, bf16[1024,2048]{1,0:T(8,128)(2,1)S(1)} %bitcast.89, bf16[1,2048,512]{2,1,0:T(8,128)(2,1)S(1)} %copy-done.11, f32[2048]{0:T(1024)S(1)} %copy-done.14, f32[1024]{0:T(1024)S(1)} %rsqrt_bitcast_fusion), kind=kOutput, calls=%fused_computation.18 | convolution fusion | flops 2154823680 | bytes 9449472 | tf_op jit(solution)/shard_map/erd,edf->erf/dot_general | solution.py:123
  191.0 50.3 %all-gather.10.cloned.1.call-done = bf16[1024,2048]{1,0:T(8,128)(2,1)} async-done(((bf16[1024,512]{1,0:T(8,128)(2,1)}), bf16[1024,2048]{1,0:T(8,128)(2,1)}) %all-gather.10.cloned.1.call-update) | async-done | bytes 4194320 | tf_op jit(solution)/shard_map/all_gather | solution.py:133
  241.3 5.5 %fusion.16 = bf16[1024,512]{1,0:T(8,128)(2,1)} fusion(bf16[1024,2048]{1,0:T(8,128)(2,1)} %all-gather.10.cloned.1.call-done, bf16[1,2048,512]{2,1,0:T(8,128)(2,1)S(1)} %copy-done), kind=kOutput, calls=%fused_computation.24 | convolution fusion | flops 2148007936 | bytes 7340032 | tf_op jit(solution)/shard_map/erf,efd->erd/dot_general | solution.py:135
  246.8 4.6 %all-to-all-start.2 = ((bf16[1,8,128,512]{3,2,0,1:T(8,128)(2,1)}), bf16[1,8,128,512]{3,2,0,1:T(8,128)(2,1)}, u32[]{:S(2)}, u32[]{:S(2)}) async-start(bf16[1,8,128,512]{3,2,0,1:T(8,128)(2,1)} %bitcast.93), calls=%async_computation.2 | async-start | bytes 2097152 | tf_op jit(solution)/shard_map/all_to_all | solution.py:140
  251.4 2.6 fusion.23
  254.0 1.6 fusion.27
  256.3 21.8 %all-to-all-done.2 = bf16[1,8,128,512]{3,2,0,1:T(8,128)(2,1)} async-done(((bf16[1,8,128,512]{3,2,0,1:T(8,128)(2,1)}), bf16[1,8,128,512]{3,2,0,1:T(8,128)(2,1)}, u32[]{:S(2)}, u32[]{:S(2)}) %all-to-all-start.2) | async-done | bytes 1048608 | tf_op jit(solution)/shard_map/all_to_all | solution.py:140
  278.0 3.3 %gather_fusion.2 = bf16[512,512]{1,0:T(8,128)(2,1)S(1)} fusion(bf16[1024,512]{1,0:T(8,128)(2,1)} %bitcast.25, s32[1024]{0:T(1024)S(1)} %pad_clamp_fusion), kind=kCustom, calls=%fused_computation.2 | custom fusion | bytes 1050624 | tf_op jit(solution)/shard_map/jit(_take)/gather | solution.py:143
  281.6 1.8 fusion.30
  283.4 3.4 %fusion.26 = bf16[256,512]{1,0:T(8,128)(2,1)} fusion(bf16[256,2048]{1,0:T(8,128)(2,1)} %all-gather.8.cloned.1.call-done, bf16[2048,512]{1,0:T(8,128)(2,1)} %param.27, f32[256,1,512]{2,1,0:T(1,128)} %fusion.30, bf16[256,512]{1,0:T(8,128)(2,1)S(1)} %copy-done.3), kind=kOutput, calls=%fused_computation.35 | convolution fusion | flops 537395200 | bytes 4194304 | tf_op jit(solution)/shard_map/dot_general | solution.py:138
  (90 shorter events, 15.6 us)
Async XLA Ops:
  6.5 234.7 %copy-start = (bf16[1,2048,512]{2,1,0:T(8,128)(2,1)S(1)}, bf16[1,2048,512]{2,1,0:T(8,128)(2,1)}, u32[]{:S(2)}) copy-start(bf16[1,2048,512]{2,1,0:T(8,128)(2,1)} %param.24) | copy-start | bytes 6291460
  7.8 5.5 %copy-start.2 = (bf16[2,256,256]{1,2,0:T(8,128)(2,1)}, bf16[2,256,256]{1,2,0:T(8,128)(2,1)S(1)}, u32[]{:S(2)}) copy-start(bf16[2,256,256]{1,2,0:T(8,128)(2,1)S(1)} %copy.63) | copy-start | bytes 786436
  7.8 10.9 %copy-start.4 = (bf16[256,256]{1,0:T(8,128)(2,1)S(1)}, bf16[256,256]{1,0:T(8,128)(2,1)}, u32[]{:S(2)}) copy-start(bf16[256,256]{1,0:T(8,128)(2,1)} %param.14) | copy-start | bytes 393220
  7.8 11.8 %collective-permute-start = (bf16[2,128,256]{1,2,0:T(8,128)(2,1)S(1)}, bf16[2,128,256]{1,2,0:T(8,128)(2,1)}, u32[]{:S(2)}, u32[]{:S(2)}) collective-permute-start(bf16[2,128,256]{1,2,0:T(8,128)(2,1)S(1)} %slice.34), channel_id=1, source_target_pairs={{0,4},{4,8},{8,12},{12,16},{16,20},{20,24},{24,28},{1,5},{5,9},{9,... | collective-permute-start | bytes 393224 | tf_op jit(solution)/shard_map/ppermute | solution.py:20
  13.3 29.4 %all-to-all-start = ((bf16[256,4,512]{0,2,1:T(8,128)(2,1)}), bf16[256,4,512]{0,2,1:T(8,128)(2,1)S(1)}, u32[]{:S(2)}, u32[]{:S(2)}) async-start(bf16[256,4,512]{0,2,1:T(8,128)(2,1)} %bitcast.91), calls=%async_computation | async-start | bytes 2097152 | tf_op jit(solution)/shard_map/all_to_all | solution.py:81
  17.8 54.0 %all-gather.6.cloned.1.call-start = ((), (), s32[]{:S(2)}) async-start(), calls=%async_computation.3 | async-start | bytes 1310720 | tf_op jit(solution)/shard_map/all_gather | solution.py:91
  22.0 5.6 %copy-start.6 = (pred[2,128,256]{1,2,0:T(8,128)(4,1)S(1)}, pred[2,128,256]{1,2,0:T(8,128)(4,1)}, u32[]{:S(2)}) copy-start(pred[2,128,256]{1,2,0:T(8,128)(4,1)} %broadcast_and_fusion) | copy-start | bytes 196612
  24.0 5.1 %copy-start.9 = (f32[4]{0:T(128)S(1)}, f32[4]{0:T(128)}, u32[]{:S(2)}) copy-start(f32[4]{0:T(128)} %param.16) | copy-start | bytes 52
  27.6 1.8 copy-start.5
  29.8 14.3 %copy-start.13 = (bf16[256,512]{1,0:T(8,128)(2,1)S(1)}, bf16[256,512]{1,0:T(8,128)(2,1)}, u32[]{:S(2)}) copy-start(bf16[256,512]{1,0:T(8,128)(2,1)} %param.18) | copy-start | bytes 786436
  42.7 4.0 %copy-start.7 = (s32[256,2]{0,1:T(2,128)S(1)}, s32[256,2]{0,1:T(2,128)}, u32[]{:S(2)}) copy-start(s32[256,2]{0,1:T(2,128)} %param.20) | copy-start | bytes 6148
  46.6 194.7 %all-gather.10.cloned.1.call-start = ((), (), s32[]{:S(2)}) async-start(), calls=%async_computation.5 | async-start | bytes 5242880 | tf_op jit(solution)/shard_map/all_gather | solution.py:133
  182.9 1.6 copy-start.10
  182.9 1.6 copy-start.14
  184.5 2.4 copy-start.11
  186.9 3.8 %copy-start.1 = (bf16[256,2048]{1,0:T(8,128)(2,1)S(1)}, bf16[256,2048]{1,0:T(8,128)(2,1)}, u32[]{:S(2)}) copy-start(bf16[256,2048]{1,0:T(8,128)(2,1)} %all-gather.6.cloned.1.call-done) | copy-start | bytes 3145732
  246.8 31.3 %all-to-all-start.2 = ((bf16[1,8,128,512]{3,2,0,1:T(8,128)(2,1)}), bf16[1,8,128,512]{3,2,0,1:T(8,128)(2,1)}, u32[]{:S(2)}, u32[]{:S(2)}) async-start(bf16[1,8,128,512]{3,2,0,1:T(8,128)(2,1)} %bitcast.93), calls=%async_computation.2 | async-start | bytes 2097152 | tf_op jit(solution)/shard_map/all_to_all | solution.py:140
  251.4 32.0 %all-gather.8.cloned.1.call-start = ((), (), s32[]{:S(2)}) async-start(), calls=%async_computation.4 | async-start | bytes 1310720 | tf_op jit(solution)/shard_map/all_gather | solution.py:134
  251.4 2.6 copy-start.12
  254.0 2.1 copy-start.8
  281.6 1.8 copy-start.3
Sparse Core Ops, SparseCore 0:
  46.7 25.0 all-gather.5
  190.8 50.3 all-gather.9
  255.8 26.7 all-gather.7
where the time goes:
time: 294 us; the launch traced here: 293 us
  blocking collectives  111 us (38%)
  waiting for transfers between devices  92.4 us (31%)
  local copies, waits for them, and re-layouts  30.1 us (10%)
  matrix products  25.3 us (9%)
  between operations  13.5 us (5%)
  starting transfers between devices  12.4 us (4%)
  other arithmetic  8.46 us (3%)
    all_to_all x1, blocking collectives, per_device(): lax.all_to_all(picked_rows.reshape(EXP_DEV, sp_count, capacity, stream_ro...  98.4 us
    all_gather x1, waiting for transfers between devices, per_device(): routed_piece = lax.all_gather(hidden, 'tp', axis=2, tiled=True)  50.3 us
    all_to_all x1, waiting for transfers between devices, per_device(): lax.all_to_all(outgoing, 'sp', split_axis=1, concat_axis=1, tiled=True)  21.8 us
    all_gather x1, waiting for transfers between devices, per_device(): stream_rows = lax.all_gather(stream_cols, 'tp', axis=1, tiled=True)  20.4 us
    all_gather x1, blocking collectives, per_device(): attended_all = lax.all_gather(attended_values, 'tp', axis=1, tiled=True)  12.7 us
    gather x1, local copies, waits for them, and re-layouts, per_device(): jnp.take(stream_rows, slot_owner, axis=0, mode='fill', fill_value=0)  10.2 us
  transfers between devices with their start and end apart: 6, of which 3 were waited for; matrix products, arithmetic and copies ran while one was open for 10% of the time, Pallas kernels for 0%

commit v1 on v0

--- a/solution.py
+++ b/solution.py
@@ -130,11 +130,23 @@
     shared_hidden = (jax.nn.silu(own_scale * shared_gate_sum) * (own_scale * shared_up_sum)).astype(
         jnp.bfloat16
     )
-    routed_piece = lax.all_gather(hidden, "tp", axis=2, tiled=True)
     own_piece = lax.all_gather(shared_hidden[None], "tp", axis=2, tiled=True)
-    expert_out = jnp.einsum(
-        "erf,efd->erd", routed_piece, down_weight, preferred_element_type=jnp.float32
-    )
+    size, index, rows = (lax.axis_size("tp"), lax.axis_index("tp"), hidden.shape[2])
+    right = [(i, (i + 1) % size) for i in range(size)]
+    held, so_far = (hidden, None)
+    for step in range(size):
+        coming = lax.ppermute(held, "tp", right) if step < size - 1 else None
+        take_in = jnp.einsum(
+            "erf,efd->erd",
+            held,
+            lax.dynamic_slice_in_dim(
+                down_weight, (index - step) % size * rows, held.shape[2], axis=1
+            ),
+            preferred_element_type=jnp.float32,
+        )
+        so_far = take_in if so_far is None else so_far + take_in
+        held = coming
+    expert_out = so_far
     shared_out = jnp.dot(own_piece[0], shared_down, preferred_element_type=jnp.float32)
     outgoing = expert_out.astype(jnp.bfloat16).reshape(EXP_DEV, sp_count, capacity, col_width)
     returned = lax.all_to_all(outgoing, "sp", split_axis=1, concat_axis=1, tiled=True).reshape(

time: 294 us -> 314 us (1.068)
  waiting for transfers between devices: 92.4 us -> 108 us
    ppermute x0 -> x3, waiting for transfers between devices: none -> 66.2 us  [per_device(): coming = lax.ppermute(held, 'tp', right) if step < size - 1 else None]
    all_gather x1 -> x0, waiting for transfers between devices: 50.3 us -> none  [per_device(): routed_piece = lax.all_gather(hidden, 'tp', axis=2, tiled=True)]
    dot_general x1 -> x4, matrix products: 5.49 us -> 7.51 us  [per_device(): jnp.einsum('erf,efd->erd', held, lax.dynamic_slice_in_dim(down_weight, (i...]
    unnamed x36 -> x38, local copies, waits for them, and re-layouts: 5.35 us -> 6.35 us
  transfers between devices with their start and end apart: 6 -> 8, of which waited for: 3 -> 5; matrix products, arithmetic and copies ran while one was open for 10% -> 11% of each run, Pallas kernels for 0% -> 0%
where the time goes in v1:
time: 314 us; the launch traced here: 313 us
  blocking collectives  111 us (35%)
  waiting for transfers between devices  108 us (34%)
  local copies, waits for them, and re-layouts  31.1 us (10%)
  matrix products  26.3 us (8%)
  starting transfers between devices  14.2 us (5%)
  between operations  13.8 us (4%)
  other arithmetic  8.48 us (3%)
    all_to_all x1, blocking collectives, per_device(): lax.all_to_all(picked_rows.reshape(EXP_DEV, sp_count, capacity, stream_ro...  98.4 us
    ppermute x3, waiting for transfers between devices, per_device(): coming = lax.ppermute(held, 'tp', right) if step < size - 1 else None  66.2 us
    all_to_all x1, waiting for transfers between devices, per_device(): lax.all_to_all(outgoing, 'sp', split_axis=1, concat_axis=1, tiled=True)  21.8 us
    all_gather x1, waiting for transfers between devices, per_device(): stream_rows = lax.all_gather(stream_cols, 'tp', axis=1, tiled=True)  20.4 us
    all_gather x1, blocking collectives, per_device(): attended_all = lax.all_gather(attended_values, 'tp', axis=1, tiled=True)  12.8 us
    gather x1, local copies, waits for them, and re-layouts, per_device(): jnp.take(stream_rows, slot_owner, axis=0, mode='fill', fill_value=0)  10.2 us
    dot_general x4, matrix products, per_device(): jnp.einsum('erf,efd->erd', held, lax.dynamic_slice_in_dim(down_weight, (i...  7.51 us
    unnamed x38, local copies, waits for them, and re-layouts  6.35 us
  transfers between devices with their start and end apart: 8, of which 5 were waited for; matrix products, arithmetic and copies ran while one was open for 11% of the time, Pallas kernels for 0%

profile of v1, /device:TPU:0, one launch (start us, length us, event | category | flops | bytes accessed | tf_op | source)
XLA Modules:
  0.0 313.3 jit_solution(9047739267193468589)
XLA Ops:
  7.8 3.2 %collective-permute-start = (bf16[2,128,256]{1,2,0:T(8,128)(2,1)S(1)}, bf16[2,128,256]{1,2,0:T(8,128)(2,1)}, u32[]{:S(2)}, u32[]{:S(2)}) collective-permute-start(bf16[2,128,256]{1,2,0:T(8,128)(2,1)S(1)} %slice.34), channel_id=1, source_target_pairs={{0,4},{4,8},{8,12},{12,16},{16,20},{20,24},{24,28},{1,5},{5,9},{9,... | collective-permute-start | bytes 393224 | tf_op jit(solution)/shard_map/ppermute | solution.py:20
  11.0 2.3 copy.73
  13.3 4.5 %all-to-all-start = ((bf16[256,4,512]{0,2,1:T(8,128)(2,1)}), bf16[256,4,512]{0,2,1:T(8,128)(2,1)S(1)}, u32[]{:S(2)}, u32[]{:S(2)}) async-start(bf16[256,4,512]{0,2,1:T(8,128)(2,1)} %bitcast.109), calls=%async_computation | async-start | bytes 2097152 | tf_op jit(solution)/shard_map/all_to_all | solution.py:81
  30.0 12.8 %all_gather.9 = bf16[256,1024]{0,1:T(8,128)(2,1)} all-gather(bf16[256,256]{0,1:T(8,128)(2,1)S(1)} %bitcast.113), channel_id=1, replica_groups=mesh['sp'=8,'tp'=4] {'tp'}, dimensions={1}, use_global_device_ids=true | all-gather | bytes 655360 | tf_op jit(solution)/shard_map/all_gather | solution.py:79
  44.1 2.6 fusion.20
  48.9 2.4 scatter_custom_fusion
  51.4 20.4 %all-gather.4.cloned.1.call-done = bf16[256,2048]{1,0:T(8,128)(2,1)} async-done(((bf16[256,512]{1,0:T(8,128)(2,1)}), bf16[256,2048]{1,0:T(8,128)(2,1)}) %all-gather.4.cloned.1.call-update) | async-done | bytes 1048592 | tf_op jit(solution)/shard_map/all_gather | solution.py:91
  71.8 10.2 %gather_fusion.1 = bf16[1024,2048]{1,0:T(8,128)(2,1)} fusion(bf16[256,2048]{1,0:T(8,128)(2,1)} %all-gather.4.cloned.1.call-done, s32[1024]{0:T(1024)S(1)} %fusion.48), kind=kCustom, calls=%fused_computation.1 | custom fusion | bytes 8392704 | tf_op jit(solution)/shard_map/jit(_take)/gather | solution.py:112
  81.9 2.5 broadcast_select_fusion
  84.5 98.4 %all_to_all.25 = bf16[1,8,128,2048]{3,2,0,1:T(8,128)(2,1)S(1)} all-to-all(bf16[1,8,128,2048]{3,2,0,1:T(8,128)(2,1)S(1)} %broadcast_select_fusion), channel_id=1, replica_groups=mesh['sp'=8,'tp'=4] {'sp'}, dimensions={1} | all-to-all | bytes 8388608 | tf_op jit(solution)/shard_map/all_to_all | solution.py:113
  184.5 2.4 fusion.3
  186.9 2.7 multiply_convert_fusion.6
  192.1 24.1 %collective-permute-done.1 = bf16[1,1024,512]{2,1,0:T(8,128)(2,1)} collective-permute-done((bf16[1,1024,512]{2,1,0:T(8,128)(2,1)S(1)}, bf16[1,1024,512]{2,1,0:T(8,128)(2,1)}, u32[]{:S(2)}, u32[]{:S(2)}) %collective-permute-start.1) | collective-permute-done | bytes 1048608 | tf_op jit(solution)/shard_map/ppermute | solution.py:138
  217.1 24.0 %collective-permute-done.2 = bf16[1,1024,512]{2,1,0:T(8,128)(2,1)} collective-permute-done((bf16[1,1024,512]{2,1,0:T(8,128)(2,1)}, bf16[1,1024,512]{2,1,0:T(8,128)(2,1)}, u32[]{:S(2)}, u32[]{:S(2)}) %collective-permute-start.2) | collective-permute-done | bytes 1048608 | tf_op jit(solution)/shard_map/ppermute | solution.py:138
  241.1 1.9 fusion.33
  243.0 1.9 fusion.27
  245.0 1.9 fusion.25
  246.9 18.1 %collective-permute-done.3 = bf16[1,1024,512]{2,1,0:T(8,128)(2,1)S(1)} collective-permute-done((bf16[1,1024,512]{2,1,0:T(8,128)(2,1)}, bf16[1,1024,512]{2,1,0:T(8,128)(2,1)S(1)}, u32[]{:S(2)}, u32[]{:S(2)}) %collective-permute-start.3) | collective-permute-done | bytes 1048608 | tf_op jit(solution)/shard_map/ppermute | solution.py:138
  266.7 4.3 %all-to-all-start.2 = ((bf16[1,8,128,512]{3,2,0,1:T(8,128)(2,1)}), bf16[1,8,128,512]{3,2,0,1:T(8,128)(2,1)}, u32[]{:S(2)}, u32[]{:S(2)}) async-start(bf16[1,8,128,512]{3,2,0,1:T(8,128)(2,1)} %bitcast.107), calls=%async_computation.2 | async-start | bytes 2097152 | tf_op jit(solution)/shard_map/all_to_all | solution.py:152
  271.2 2.6 fusion.18
  276.0 21.8 %all-to-all-done.2 = bf16[1,8,128,512]{3,2,0,1:T(8,128)(2,1)} async-done(((bf16[1,8,128,512]{3,2,0,1:T(8,128)(2,1)}), bf16[1,8,128,512]{3,2,0,1:T(8,128)(2,1)}, u32[]{:S(2)}, u32[]{:S(2)}) %all-to-all-start.2) | async-done | bytes 1048608 | tf_op jit(solution)/shard_map/all_to_all | solution.py:152
  297.8 3.3 %gather_fusion.2 = bf16[512,512]{1,0:T(8,128)(2,1)S(1)} fusion(bf16[1024,512]{1,0:T(8,128)(2,1)} %bitcast.32, s32[1024]{0:T(1024)S(1)} %pad_clamp_fusion), kind=kCustom, calls=%fused_computation.2 | custom fusion | bytes 1050624 | tf_op jit(solution)/shard_map/jit(_take)/gather | solution.py:155
  301.3 1.8 fusion.39
  303.1 3.4 %fusion.21 = bf16[256,512]{1,0:T(8,128)(2,1)} fusion(bf16[256,2048]{1,0:T(8,128)(2,1)} %all-gather.6.cloned.1.call-done, bf16[2048,512]{1,0:T(8,128)(2,1)} %param.27, f32[256,1,512]{2,1,0:T(1,128)} %fusion.39, bf16[256,512]{1,0:T(8,128)(2,1)S(1)} %copy-done.4), kind=kOutput, calls=%fused_computation.33 | convolution fusion | flops 537395200 | bytes 4194304 | tf_op jit(solution)/shard_map/dot_general | solution.py:150
  (98 shorter events, 26.0 us)
Async XLA Ops:
  6.5 234.6 %copy-start = (bf16[1,2048,512]{2,1,0:T(8,128)(2,1)S(1)}, bf16[1,2048,512]{2,1,0:T(8,128)(2,1)}, u32[]{:S(2)}) copy-start(bf16[1,2048,512]{2,1,0:T(8,128)(2,1)} %param.24) | copy-start | bytes 6291460
  7.8 5.5 %copy-start.3 = (bf16[2,256,256]{1,2,0:T(8,128)(2,1)}, bf16[2,256,256]{1,2,0:T(8,128)(2,1)S(1)}, u32[]{:S(2)}) copy-start(bf16[2,256,256]{1,2,0:T(8,128)(2,1)S(1)} %copy.63) | copy-start | bytes 786436
  7.8 11.0 %copy-start.5 = (bf16[256,256]{1,0:T(8,128)(2,1)S(1)}, bf16[256,256]{1,0:T(8,128)(2,1)}, u32[]{:S(2)}) copy-start(bf16[256,256]{1,0:T(8,128)(2,1)} %param.14) | copy-start | bytes 393220
  7.8 11.8 %collective-permute-start = (bf16[2,128,256]{1,2,0:T(8,128)(2,1)S(1)}, bf16[2,128,256]{1,2,0:T(8,128)(2,1)}, u32[]{:S(2)}, u32[]{:S(2)}) collective-permute-start(bf16[2,128,256]{1,2,0:T(8,128)(2,1)S(1)} %slice.34), channel_id=1, source_target_pairs={{0,4},{4,8},{8,12},{12,16},{16,20},{20,24},{24,28},{1,5},{5,9},{9,... | collective-permute-start | bytes 393224 | tf_op jit(solution)/shard_map/ppermute | solution.py:20
  13.3 29.5 %all-to-all-start = ((bf16[256,4,512]{0,2,1:T(8,128)(2,1)}), bf16[256,4,512]{0,2,1:T(8,128)(2,1)S(1)}, u32[]{:S(2)}, u32[]{:S(2)}) async-start(bf16[256,4,512]{0,2,1:T(8,128)(2,1)} %bitcast.109), calls=%async_computation | async-start | bytes 2097152 | tf_op jit(solution)/shard_map/all_to_all | solution.py:81
  17.8 54.0 %all-gather.4.cloned.1.call-start = ((), (), s32[]{:S(2)}) async-start(), calls=%async_computation.3 | async-start | bytes 1310720 | tf_op jit(solution)/shard_map/all_gather | solution.py:91
  22.0 5.6 %copy-start.7 = (pred[2,128,256]{1,2,0:T(8,128)(4,1)S(1)}, pred[2,128,256]{1,2,0:T(8,128)(4,1)}, u32[]{:S(2)}) copy-start(pred[2,128,256]{1,2,0:T(8,128)(4,1)} %broadcast_and_fusion) | copy-start | bytes 196612
  24.1 5.1 %copy-start.10 = (f32[4]{0:T(128)S(1)}, f32[4]{0:T(128)}, u32[]{:S(2)}) copy-start(f32[4]{0:T(128)} %param.16) | copy-start | bytes 52
  27.7 1.8 copy-start.6
  29.8 14.3 %copy-start.14 = (bf16[256,512]{1,0:T(8,128)(2,1)S(1)}, bf16[256,512]{1,0:T(8,128)(2,1)}, u32[]{:S(2)}) copy-start(bf16[256,512]{1,0:T(8,128)(2,1)} %param.18) | copy-start | bytes 786436
  42.7 3.9 %copy-start.8 = (s32[256,2]{0,1:T(2,128)S(1)}, s32[256,2]{0,1:T(2,128)}, u32[]{:S(2)}) copy-start(s32[256,2]{0,1:T(2,128)} %param.20) | copy-start | bytes 6148
  182.9 1.6 copy-start.11
  182.9 1.6 copy-start.15
  184.5 2.4 copy-start.12
  186.9 29.9 %copy-start.1 = (bf16[256,2048]{1,0:T(8,128)(2,1)S(1)}, bf16[256,2048]{1,0:T(8,128)(2,1)}, u32[]{:S(2)}) copy-start(bf16[256,2048]{1,0:T(8,128)(2,1)} %all-gather.4.cloned.1.call-done) | copy-start | bytes 3145732
  189.7 1.0 copy-start.2
  190.7 25.5 %collective-permute-start.1 = (bf16[1,1024,512]{2,1,0:T(8,128)(2,1)S(1)}, bf16[1,1024,512]{2,1,0:T(8,128)(2,1)}, u32[]{:S(2)}, u32[]{:S(2)}) collective-permute-start(bf16[1,1024,512]{2,1,0:T(8,128)(2,1)S(1)} %bitcast.111), channel_id=1, source_target_pairs={{0,1},{1,2},{2,3},{3,0},{4,5},{5,6},{6,7},{7,4},{8,9},{9,10},{10,1... | collective-permute-start | bytes 3145736 | tf_op jit(solution)/shard_map/ppermute | solution.py:138
  216.2 24.9 %collective-permute-start.2 = (bf16[1,1024,512]{2,1,0:T(8,128)(2,1)}, bf16[1,1024,512]{2,1,0:T(8,128)(2,1)}, u32[]{:S(2)}, u32[]{:S(2)}) collective-permute-start(bf16[1,1024,512]{2,1,0:T(8,128)(2,1)} %collective-permute-done.1), channel_id=1, source_target_pairs={{0,1},{1,2},{2,3},{3,0},{4,5},{5,6},{6,7},{7,4},{8,9},{9,10},{10,1... | collective-permute-start | bytes 3145736 | tf_op jit(solution)/shard_map/ppermute | solution.py:138
  241.1 23.9 %collective-permute-start.3 = (bf16[1,1024,512]{2,1,0:T(8,128)(2,1)}, bf16[1,1024,512]{2,1,0:T(8,128)(2,1)S(1)}, u32[]{:S(2)}, u32[]{:S(2)}) collective-permute-start(bf16[1,1024,512]{2,1,0:T(8,128)(2,1)} %collective-permute-done.2), channel_id=1, source_target_pairs={{0,1},{1,2},{2,3},{3,0},{4,5},{5,6},{6,7},{7,4},{8,9},{9,10},{10,1... | collective-permute-start | bytes 3145736 | tf_op jit(solution)/shard_map/ppermute | solution.py:138
  266.7 31.0 %all-to-all-start.2 = ((bf16[1,8,128,512]{3,2,0,1:T(8,128)(2,1)}), bf16[1,8,128,512]{3,2,0,1:T(8,128)(2,1)}, u32[]{:S(2)}, u32[]{:S(2)}) async-start(bf16[1,8,128,512]{3,2,0,1:T(8,128)(2,1)} %bitcast.107), calls=%async_computation.2 | async-start | bytes 2097152 | tf_op jit(solution)/shard_map/all_to_all | solution.py:152
  271.1 32.0 %all-gather.6.cloned.1.call-start = ((), (), s32[]{:S(2)}) async-start(), calls=%async_computation.4 | async-start | bytes 1310720 | tf_op jit(solution)/shard_map/all_gather | solution.py:133
  271.1 2.6 copy-start.13
  273.7 2.1 copy-start.9
  301.3 1.8 copy-start.4
Sparse Core Ops, SparseCore 0:
  46.8 24.9 all-gather.3
  275.5 26.7 all-gather.5
